TPU v7x, 32 devices: a whole 2x2x4 slice. The times are simulated.
32 devices in a mesh: tp: 8 (over z, core), dp: 4 (over y, x).
Axes of the slice: x: 2, y: 2, z: 4, core: 2. Of those that a mesh axis runs over, the one named last changes fastest.
Arguments:
- tokens: bfloat16 [32, 4096], P('tp', 'dp'), may hold values from -6 to 6
- norm_gain: bfloat16 [2, 4096], P(None, 'dp'), may hold values from 0.099609375 to 1.8984375
- w_query: bfloat16 [2, 4096, 1024], P(None, 'dp', 'tp'), may hold values from -0.09375 to 0.09375
- w_key: bfloat16 [2, 4096, 1024], P(None, 'dp', 'tp'), may hold values from -0.09375 to 0.09375
- w_value: bfloat16 [2, 4096, 1024], P(None, 'dp', 'tp'), may hold values from -0.09375 to 0.09375
- w_outgate: bfloat16 [2, 4096, 1024], P(None, 'dp', 'tp'), may hold values from -0.09375 to 0.09375
- w_gates: bfloat16 [2, 4096, 16], P(None, 'dp'), may hold values from -0.09375 to 0.09375
- gate_bias: float32 [2, 2, 8], P(None, None, 'tp'), may hold values from -1 to 5
- w_out: bfloat16 [2, 1024, 4096], P(None, 'tp', 'dp'), may hold values from -0.1875 to 0.1875
- memory: float32 [2, 32, 8, 128, 128], P(None, 'dp', 'tp'), may hold values from -6 to 6
- normalizer: float32 [2, 32, 8, 128], P(None, 'dp', 'tp'), may hold values from -3 to 3
- stabilizer: float32 [2, 32, 8], P(None, 'dp', 'tp'), may hold values from -8 to 300, as said below
Outputs:
- mixed: bfloat16 [32, 4096], P('tp', 'dp')
- new_memory: float32 [2, 32, 8, 128, 128], P(None, 'dp', 'tp')
- new_normalizer: float32 [2, 32, 8, 128], P(None, 'dp', 'tp')
- new_stabilizer: float32 [2, 32, 8], P(None, 'dp', 'tp')
Inputs may be any that keep to these rules, and one draw needn't show every extreme that they name: `stabilizer`: lies between -8 and 8, except that some entries may be as large as 300.
All inputs are finite; a program needn't handle non-finite values.
Results may differ from a plain program's by a relative error of at most 0.04.
Values may be sent and summed in bfloat16 or wider, within the bound.
A program may use at most 64 MiB of HBM per device.

v0:
```python
import jax
import jax.numpy as jnp
from jax import lax
from jax.sharding import PartitionSpec as P

D = 4096
HEAD_SIZE = 128
epsilon = 1e-06


def cell_update(query, key_rows, value_rows, input_pre, forget_pre, memory, normalizer, stabilizer):
    batch_size = query.shape[0]
    head_count = input_pre.shape[1]
    query_float = query.astype(jnp.float32).reshape(batch_size, head_count, -1)
    key_float = key_rows.astype(jnp.float32).reshape(
        batch_size, head_count, -1
    ) * query_float.shape[2] ** (-0.5)
    value_float = value_rows.astype(jnp.float32).reshape(batch_size, head_count, -1)
    carried = jax.nn.log_sigmoid(forget_pre) + stabilizer
    new_max = jnp.maximum(carried, input_pre)
    keep_factor = jnp.exp(carried - new_max)
    write_factor = jnp.exp(input_pre - new_max)
    new_memory = (
        keep_factor[:, :, None, None] * memory
        + write_factor[:, :, None, None] * value_float[:, :, :, None] * key_float[:, :, None, :]
    )
    new_normalizer = keep_factor[:, :, None] * normalizer + write_factor[:, :, None] * key_float
    numerator = jnp.sum(new_memory * query_float[:, :, None, :], axis=3)
    denominator = jnp.sum(new_normalizer * query_float, axis=2)
    floor_value = jnp.maximum(jnp.abs(denominator), jnp.exp(-new_max))
    readout = numerator / jnp.maximum(floor_value, 1.0)[:, :, None]
    return (readout.reshape(batch_size, -1), new_memory, new_normalizer, new_max)


def finish_split(partial_out, wide_rows):
    summed = lax.psum_scatter(partial_out, "tp", scatter_dimension=0, tiled=True)
    own_rows = lax.dynamic_slice_in_dim(
        wide_rows, lax.axis_index("tp") * summed.shape[0], summed.shape[0], 0
    )
    return (own_rows + summed).astype(jnp.bfloat16)


def body(
    tokens,
    norm_gain,
    w_query,
    w_key,
    w_value,
    w_outgate,
    w_gates,
    gate_bias,
    w_out,
    memory,
    normalizer,
    stabilizer,
):
    heads_here = w_query.shape[2] // HEAD_SIZE
    seq_here = memory.shape[1]
    all_heads = w_gates.shape[2] // 2
    head_first = lax.axis_index("tp") * heads_here
    seq_first = lax.axis_index("dp") * seq_here
    current = tokens
    gathered = None
    memories = []
    normalizers = []
    maxima = []
    for layer_index in range(2):
        if gathered is None:
            gathered = lax.all_gather(current, "tp", axis=0, tiled=True)
        wide_rows = gathered.astype(jnp.float32)
        square_part = jnp.sum(wide_rows * wide_rows, axis=1)
        scaled = (wide_rows * norm_gain[layer_index].astype(jnp.float32)[None, :]).astype(
            jnp.bfloat16
        )
        gate_weight = w_gates[layer_index]
        own_gates = jnp.concatenate(
            [
                lax.dynamic_slice_in_dim(gate_weight, head_first, heads_here, 1),
                lax.dynamic_slice_in_dim(gate_weight, all_heads + head_first, heads_here, 1),
            ],
            axis=1,
        )
        term_query = jnp.dot(scaled, w_query[layer_index], preferred_element_type=jnp.float32)
        term_key = jnp.dot(scaled, w_key[layer_index], preferred_element_type=jnp.float32)
        term_value = jnp.dot(scaled, w_value[layer_index], preferred_element_type=jnp.float32)
        term_outgate = jnp.dot(scaled, w_outgate[layer_index], preferred_element_type=jnp.float32)
        term_gates = jnp.dot(scaled, own_gates, preferred_element_type=jnp.float32)
        square_all = lax.psum(square_part, "dp")
        square_own = lax.dynamic_slice_in_dim(square_all, seq_first, seq_here, 0)
        sum_query, sum_key, sum_value, sum_outgate, sum_gates = (
            lax.psum_scatter(term_query, "dp", scatter_dimension=0, tiled=True),
            lax.psum_scatter(term_key, "dp", scatter_dimension=0, tiled=True),
            lax.psum_scatter(term_value, "dp", scatter_dimension=0, tiled=True),
            lax.psum_scatter(term_outgate, "dp", scatter_dimension=0, tiled=True),
            lax.psum_scatter(term_gates, "dp", scatter_dimension=0, tiled=True),
        )
        inv_scale = lax.rsqrt(square_own / D + epsilon)[:, None]
        query = (sum_query * inv_scale).astype(jnp.bfloat16)
        key_rows = (sum_key * inv_scale).astype(jnp.bfloat16)
        value_rows = (sum_value * inv_scale).astype(jnp.bfloat16)
        outgate = (sum_outgate * inv_scale).astype(jnp.bfloat16)
        gate_pre = sum_gates * inv_scale
        bias_here = gate_bias[layer_index]
        input_pre = gate_pre[:, :heads_here] + bias_here[0][None, :]
        forget_pre = gate_pre[:, heads_here:] + bias_here[1][None, :]
        readout, new_memory, new_normalizer, new_max = cell_update(
            query,
            key_rows,
            value_rows,
            input_pre,
            forget_pre,
            memory[layer_index],
            normalizer[layer_index],
            stabilizer[layer_index],
        )
        gated = (jax.nn.sigmoid(outgate.astype(jnp.float32)) * readout).astype(jnp.bfloat16)
        out_weight = w_out[layer_index]
        partial_out = jnp.dot(
            lax.all_gather(gated, "dp", axis=0, tiled=True),
            out_weight,
            preferred_element_type=jnp.float32,
        )
        if layer_index == 0:
            summed = lax.psum(partial_out, "tp")
            gathered = (wide_rows + summed).astype(jnp.bfloat16)
        else:
            current = finish_split(partial_out, wide_rows)
        memories.append(new_memory)
        normalizers.append(new_normalizer)
        maxima.append(new_max)
    return (current, jnp.stack(memories), jnp.stack(normalizers), jnp.stack(maxima))


def solution(mesh):
    placed = (
        P("tp", "dp"),
        P(None, "dp"),
        P(None, "dp", "tp"),
        P(None, "dp", "tp"),
        P(None, "dp", "tp"),
        P(None, "dp", "tp"),
        P(None, "dp", None),
        P(None, None, "tp"),
        P(None, "tp", "dp"),
        P(None, "dp", "tp", None, None),
        P(None, "dp", "tp", None),
        P(None, "dp", "tp"),
    )
    return jax.shard_map(
        body,
        mesh=mesh,
        in_specs=placed,
        out_specs=(
            P("tp", "dp"),
            P(None, "dp", "tp", None, None),
            P(None, "dp", "tp", None),
            P(None, "dp", "tp"),
        ),
        check_vma=False,
    )
```

profile of v0, /device:TPU:0, one launch (start us, length us, event | category | flops | bytes accessed | tf_op | source)
XLA Modules:
  0.0 269.4 jit_solution(6725401215718095154)
XLA Ops:
  7.2 0.8 slice_convert_fusion
  8.0 15.9 %all-gather = bf16[8,4,1024]{2,1,0:T(4,128)(2,1)S(1)} all-gather(bf16[1,4,1024]{2,1,0:T(4,128)(2,1)} %bitcast.146), channel_id=1, replica_groups=mesh['tp'=8,'dp'=4] {'tp'}, dimensions={0}, use_global_device_ids=true | all-gather | bytes 73728 | tf_op jit(solution)/shard_map/all_gather | solution.py:69
  24.6 1.7 fusion.18
  26.3 0.8 fusion.20
  27.1 0.8 fusion.22
  27.9 1.8 fusion.24
  29.7 0.7 fusion.42
  32.4 40.8 %all-reduce.24.cloned.1.call-done = (f32[32,128]{1,0:T(8,128)}, f32[32]{0:T(128)}, f32[32,128]{1,0:T(8,128)}, f32[32,128]{1,0:T(8,128)}, f32[32,2]{0,1:T(2,128)}, /*index=5*/f32[32,128]{1,0:T(8,128)}) async-done(((f32[32,128]{1,0:T(8,128)}, f32[32]{0:T(128)}, f32[32,128]{1,0:T(8,128)}, f32[32,128]{1,0:T(8,128)}, f32[32,2]{0,1:T(2,128)}, /*index=5*/f32[32,128]{1,0:T(8,128)}), (f32[32,128]{1,0:T(8,128)}, ...) | async-done | bytes 65936
  73.2 0.7 add_rsqrt_fusion.1
  74.0 0.7 fusion.62
  74.7 1.4 broadcast_multiply_fusion.1
  76.1 0.8 fusion.59
  76.8 0.9 multiply_reduce_fusion.3
  78.1 0.8 multiply_convert_fusion.3
  78.9 8.9 %all_gather.10 = bf16[32,128]{1,0:T(8,128)(2,1)S(1)} all-gather(bf16[8,128]{1,0:T(8,128)(2,1)S(1)} %multiply_convert_fusion.3), channel_id=1, replica_groups=mesh['tp'=8,'dp'=4] {'dp'}, dimensions={0}, use_global_device_ids=true | all-gather | bytes 10240 | tf_op jit(solution)/shard_map/all_gather | solution.py:119
  87.8 0.8 fusion.16
  88.7 55.4 %all-reduce.18.cloned.1.call-done = f32[32,1024]{1,0:T(8,128)} async-done(((f32[32,1024]{1,0:T(8,128)}), f32[32,1024]{1,0:T(8,128)}) %all-reduce.18.cloned.1.call-update) | async-done | bytes 131088 | tf_op jit(solution)/shard_map/psum | solution.py:124
  144.1 1.5 multiply_reduce_fusion
  145.7 0.8 fusion.8
  146.5 0.8 fusion.10
  147.2 0.8 fusion.12
  148.0 0.8 fusion.14
  151.4 38.9 %all-reduce.22.cloned.1.call-done = (f32[32,128]{1,0:T(8,128)}, f32[32]{0:T(128)}, f32[32,128]{1,0:T(8,128)}, f32[32,128]{1,0:T(8,128)}, f32[32,2]{0,1:T(2,128)}, /*index=5*/f32[32,128]{1,0:T(8,128)}) async-done(((f32[32,128]{1,0:T(8,128)}, f32[32]{0:T(128)}, f32[32,128]{1,0:T(8,128)}, f32[32,128]{1,0:T(8,128)}, f32[32,2]{0,1:T(2,128)}, /*index=5*/f32[32,128]{1,0:T(8,128)}), (f32[32,128]{1,0:T(8,128)}, ...) | async-done | bytes 65936
  191.8 1.3 broadcast_multiply_fusion
  193.1 0.8 fusion.58
  193.9 0.9 multiply_reduce_fusion.2
  195.6 0.8 multiply_convert_fusion.2
  196.3 8.9 %all_gather.11 = bf16[32,128]{1,0:T(8,128)(2,1)S(1)} all-gather(bf16[8,128]{1,0:T(8,128)(2,1)S(1)} %multiply_convert_fusion.2), channel_id=1, replica_groups=mesh['tp'=8,'dp'=4] {'dp'}, dimensions={0}, use_global_device_ids=true | all-gather | bytes 10240 | tf_op jit(solution)/shard_map/all_gather | solution.py:119
  205.2 0.8 fusion.6
  206.7 1.1 pad_maximum_fusion
  208.3 53.2 %all-reduce.20.cloned.1.call-done = f32[32,1024]{1,0:T(8,128)} async-done(((f32[32,1024]{1,0:T(8,128)}), f32[32,1024]{1,0:T(8,128)}) %all-reduce.20.cloned.1.call-update) | async-done | bytes 131088
  261.5 1.4 fusion.37
  (57 shorter events, 8.0 us)
Async XLA Ops:
  7.2 19.1 %copy-start.2 = (bf16[2,1024,128]{2,1,0:T(8,128)(2,1)S(1)}, bf16[2,1024,128]{2,1,0:T(8,128)(2,1)}, u32[]{:S(2)}) copy-start(bf16[2,1024,128]{2,1,0:T(8,128)(2,1)} %param.15) | copy-start | bytes 1572868
  7.2 66.0 %all-reduce.24.cloned.1.call-start = ((), (), s32[]{:S(2)}) async-start(), calls=%async_computation.3 | async-start | bytes 134144
  23.9 3.2 %copy-start.3 = (bf16[2,1024,128]{2,1,0:T(8,128)(2,1)S(1)}, bf16[2,1024,128]{2,1,0:T(8,128)(2,1)}, u32[]{:S(2)}) copy-start(bf16[2,1024,128]{2,1,0:T(8,128)(2,1)} %param.16) | copy-start | bytes 1572868
  23.9 5.7 %copy-start.6 = (bf16[2,1024,16]{1,2,0:T(8,128)(2,1)S(1)}, bf16[2,1024,16]{1,2,0:T(8,128)(2,1)}, u32[]{:S(2)}) copy-start(bf16[2,1024,16]{1,2,0:T(8,128)(2,1)} %param.18) | copy-start | bytes 196612
  23.9 53.8 %copy-start = (f32[2,8,1,128,128]{4,3,2,1,0:T(8,128)S(1)}, f32[2,8,1,128,128]{4,3,2,1,0:T(8,128)}, u32[]{:S(2)}) copy-start(f32[2,8,1,128,128]{4,3,2,1,0:T(8,128)} %param.21) | copy-start | bytes 3145732
  27.8 2.6 copy-start.13
  27.9 3.9 %copy-start.8 = (f32[2,2,1]{1,2,0:T(1,128)S(1)}, f32[2,2,1]{1,2,0:T(1,128)}, u32[]{:S(2)}) copy-start(f32[2,2,1]{1,2,0:T(1,128)} %param.19) | copy-start | bytes 52
  27.9 46.8 %copy-start.9 = (f32[2,8,1]{1,2,0:T(1,128)S(1)}, f32[2,8,1]{1,2,0:T(1,128)}, u32[]{:S(2)}) copy-start(f32[2,8,1]{1,2,0:T(1,128)} %param.23) | copy-start | bytes 196
  27.9 48.2 %copy-start.7 = (f32[2,8,1,128]{3,2,1,0:T(1,128)S(1)}, f32[2,8,1,128]{3,2,1,0:T(1,128)}, u32[]{:S(2)}) copy-start(f32[2,8,1,128]{3,2,1,0:T(1,128)} %param.22) | copy-start | bytes 24580
  29.6 58.1 %copy-start.5 = (bf16[2,128,1024]{2,1,0:T(8,128)(2,1)S(1)}, bf16[2,128,1024]{2,1,0:T(8,128)(2,1)}, u32[]{:S(2)}) copy-start(bf16[2,128,1024]{2,1,0:T(8,128)(2,1)} %param.20) | copy-start | bytes 1572868
  30.4 113.7 %all-reduce.18.cloned.1.call-start = ((), (), s32[]{:S(2)}) async-start(), calls=%async_computation | async-start | bytes 262144 | tf_op jit(solution)/shard_map/psum | solution.py:124
  87.8 57.9 %copy-start.1 = (bf16[2,1024,128]{2,1,0:T(8,128)(2,1)S(1)}, bf16[2,1024,128]{2,1,0:T(8,128)(2,1)}, u32[]{:S(2)}) copy-start(bf16[2,1024,128]{2,1,0:T(8,128)(2,1)} %param.14) | copy-start | bytes 1572868
  88.6 101.7 %all-reduce.22.cloned.1.call-start = ((), (), s32[]{:S(2)}) async-start(), calls=%async_computation.2 | async-start | bytes 134144
  145.7 2.3 copy-start.4
  149.5 112.0 %all-reduce.20.cloned.1.call-start = ((), (), s32[]{:S(2)}) async-start(), calls=%async_computation.1 | async-start | bytes 262144
  149.5 0.7 copy-start.12
  190.4 0.7 copy-start.11
  191.1 0.6 copy-start.10
Sparse Core Ops, SparseCore 0:
  30.5 42.6 all-reduce.23
  88.8 55.2 all-reduce.17
  149.6 40.6 all-reduce.21
  206.2 55.2 all-reduce.19
where the time goes:
time: 270 us; the launch traced here: 269 us
  waiting for transfers between devices  188 us (70%)
  blocking collectives  33.7 us (12%)
  other arithmetic  16.8 us (6%)
  between operations  15.2 us (6%)
  matrix products  11.1 us (4%)
  local copies, waits for them, and re-layouts  3.91 us (1%)
    unnamed x7, waiting for transfers between devices  133 us
    psum x1, waiting for transfers between devices, body(): summed = lax.psum(partial_out, 'tp')  55.4 us
    all_gather x2, blocking collectives, body(): lax.all_gather(gated, 'dp', axis=0, tiled=True)  17.8 us
    all_gather x1, blocking collectives, body(): gathered = lax.all_gather(current, 'tp', axis=0, tiled=True)  15.9 us
  transfers between devices with their start and end apart: 4, of which 4 were waited for; matrix products, arithmetic and copies ran while one was open for 2% of the time, Pallas kernels for 0%

commit v1 on v0

--- a/solution.py
+++ b/solution.py
@@ -121,7 +121,7 @@
             preferred_element_type=jnp.float32,
         )
         if layer_index == 0:
-            summed = lax.psum(partial_out, "tp")
+            summed = jnp.sum(lax.all_gather(partial_out, "tp"), axis=0)
             gathered = (wide_rows + summed).astype(jnp.bfloat16)
         else:
             current = finish_split(partial_out, wide_rows)

time: 270 us -> 239 us (0.89)
  waiting for transfers between devices: 188 us -> 156 us
    psum x1 -> x0, waiting for transfers between devices: 55.4 us -> none  [body(): summed = lax.psum(partial_out, 'tp')]
    all_gather x0 -> x1, waiting for transfers between devices: none -> 22.7 us  [body(): summed = jnp.sum(lax.all_gather(partial_out, 'tp'), axis=0)]
where the time goes in v1:
time: 239 us; the launch traced here: 238 us
  waiting for transfers between devices  156 us (65%)
  blocking collectives  33.7 us (14%)
  other arithmetic  17.2 us (7%)
  between operations  15.2 us (6%)
  matrix products  11.2 us (5%)
  local copies, waits for them, and re-layouts  4.3 us (2%)
    unnamed x7, waiting for transfers between devices  134 us
    all_gather x1, waiting for transfers between devices, body(): summed = jnp.sum(lax.all_gather(partial_out, 'tp'), axis=0)  22.7 us
    all_gather x2, blocking collectives, body(): lax.all_gather(gated, 'dp', axis=0, tiled=True)  17.8 us
    all_gather x1, blocking collectives, body(): gathered = lax.all_gather(current, 'tp', axis=0, tiled=True)  15.9 us
  transfers between devices with their start and end apart: 4, of which 4 were waited for; matrix products, arithmetic and copies ran while one was open for 2% of the time, Pallas kernels for 0%

profile of v1, /device:TPU:0, one launch (start us, length us, event | category | flops | bytes accessed | tf_op | source)
XLA Modules:
  0.0 238.1 jit_solution(6166163460917791186)
XLA Ops:
  7.2 0.8 slice_convert_fusion
  8.0 15.9 %all-gather.1 = bf16[8,4,1024]{2,1,0:T(4,128)(2,1)S(1)} all-gather(bf16[1,4,1024]{2,1,0:T(4,128)(2,1)} %bitcast.148), channel_id=1, replica_groups=mesh['tp'=8,'dp'=4] {'tp'}, dimensions={0}, use_global_device_ids=true | all-gather | bytes 73728 | tf_op jit(solution)/shard_map/all_gather | solution.py:69
  24.6 1.7 fusion.18
  26.3 0.8 fusion.20
  27.1 0.8 fusion.22
  27.9 1.8 fusion.24
  29.7 0.7 fusion.42
  32.4 40.8 %all-reduce.21.cloned.1.call-done = (f32[32,128]{1,0:T(8,128)}, f32[32]{0:T(128)}, f32[32,128]{1,0:T(8,128)}, f32[32,128]{1,0:T(8,128)}, f32[32,2]{0,1:T(2,128)}, /*index=5*/f32[32,128]{1,0:T(8,128)}) async-done(((f32[32,128]{1,0:T(8,128)}, f32[32]{0:T(128)}, f32[32,128]{1,0:T(8,128)}, f32[32,128]{1,0:T(8,128)}, f32[32,2]{0,1:T(2,128)}, /*index=5*/f32[32,128]{1,0:T(8,128)}), (f32[32,128]{1,0:T(8,128)}, ...) | async-done | bytes 65936
  73.2 0.7 add_rsqrt_fusion.1
  74.0 0.7 fusion.62
  74.7 1.4 broadcast_multiply_fusion.1
  76.1 0.8 fusion.59
  76.8 0.9 multiply_reduce_fusion.3
  78.1 0.8 multiply_convert_fusion.3
  78.9 8.9 %all_gather.16 = bf16[32,128]{1,0:T(8,128)(2,1)S(1)} all-gather(bf16[8,128]{1,0:T(8,128)(2,1)S(1)} %multiply_convert_fusion.3), channel_id=1, replica_groups=mesh['tp'=8,'dp'=4] {'dp'}, dimensions={0}, use_global_device_ids=true | all-gather | bytes 10240 | tf_op jit(solution)/shard_map/all_gather | solution.py:119
  87.8 0.8 fusion.16
  88.7 22.7 %all-gather.4.cloned.1.call-done = f32[256,1024]{1,0:T(8,128)} async-done(((f32[32,1024]{1,0:T(8,128)}), f32[256,1024]{1,0:T(8,128)}) %all-gather.4.cloned.1.call-update) | async-done | bytes 1048592 | tf_op jit(solution)/shard_map/all_gather | solution.py:124
  111.4 1.3 reduce_sum.66
  113.7 0.8 fusion.8
  114.5 0.8 fusion.10
  115.3 0.8 fusion.12
  116.1 0.8 fusion.14
  119.5 39.5 %all-reduce.19.cloned.1.call-done = (f32[32,128]{1,0:T(8,128)}, f32[32]{0:T(128)}, f32[32,128]{1,0:T(8,128)}, f32[32,128]{1,0:T(8,128)}, f32[32,2]{0,1:T(2,128)}, /*index=5*/f32[32,128]{1,0:T(8,128)}) async-done(((f32[32,128]{1,0:T(8,128)}, f32[32]{0:T(128)}, f32[32,128]{1,0:T(8,128)}, f32[32,128]{1,0:T(8,128)}, f32[32,2]{0,1:T(2,128)}, /*index=5*/f32[32,128]{1,0:T(8,128)}), (f32[32,128]{1,0:T(8,128)}, ...) | async-done | bytes 65936
  160.4 1.3 broadcast_multiply_fusion
  161.7 0.8 fusion.58
  162.5 0.9 multiply_reduce_fusion.2
  164.2 0.8 multiply_convert_fusion.2
  165.0 8.9 %all_gather.19 = bf16[32,128]{1,0:T(8,128)(2,1)S(1)} all-gather(bf16[8,128]{1,0:T(8,128)(2,1)S(1)} %multiply_convert_fusion.2), channel_id=1, replica_groups=mesh['tp'=8,'dp'=4] {'dp'}, dimensions={0}, use_global_device_ids=true | all-gather | bytes 10240 | tf_op jit(solution)/shard_map/all_gather | solution.py:119
  173.9 0.8 fusion.6
  175.3 1.1 pad_maximum_fusion
  176.9 53.2 %all-reduce.17.cloned.1.call-done = f32[32,1024]{1,0:T(8,128)} async-done(((f32[32,1024]{1,0:T(8,128)}), f32[32,1024]{1,0:T(8,128)}) %all-reduce.17.cloned.1.call-update) | async-done | bytes 131088
  230.2 1.4 fusion.37
  (60 shorter events, 9.1 us)
Async XLA Ops:
  7.2 19.1 %copy-start.2 = (bf16[2,1024,128]{2,1,0:T(8,128)(2,1)S(1)}, bf16[2,1024,128]{2,1,0:T(8,128)(2,1)}, u32[]{:S(2)}) copy-start(bf16[2,1024,128]{2,1,0:T(8,128)(2,1)} %param.15) | copy-start | bytes 1572868
  7.2 66.1 %all-reduce.21.cloned.1.call-start = ((), (), s32[]{:S(2)}) async-start(), calls=%async_computation.3 | async-start | bytes 134144
  23.9 3.2 %copy-start.3 = (bf16[2,1024,128]{2,1,0:T(8,128)(2,1)S(1)}, bf16[2,1024,128]{2,1,0:T(8,128)(2,1)}, u32[]{:S(2)}) copy-start(bf16[2,1024,128]{2,1,0:T(8,128)(2,1)} %param.16) | copy-start | bytes 1572868
  23.9 5.7 %copy-start.7 = (bf16[2,1024,16]{1,2,0:T(8,128)(2,1)S(1)}, bf16[2,1024,16]{1,2,0:T(8,128)(2,1)}, u32[]{:S(2)}) copy-start(bf16[2,1024,16]{1,2,0:T(8,128)(2,1)} %param.18) | copy-start | bytes 196612
  23.9 53.8 %copy-start = (f32[2,8,1,128,128]{4,3,2,1,0:T(8,128)S(1)}, f32[2,8,1,128,128]{4,3,2,1,0:T(8,128)}, u32[]{:S(2)}) copy-start(f32[2,8,1,128,128]{4,3,2,1,0:T(8,128)} %param.21) | copy-start | bytes 3145732
  27.8 2.6 %copy-start.14 = (u32[32]{0:T(128)S(1)}, u32[32]{0:T(128)}, u32[]{:S(2)}) copy-start(u32[32]{0:T(128)} %constant.49) | copy-start | bytes 388
  27.8 3.9 %copy-start.9 = (f32[2,2,1]{1,2,0:T(1,128)S(1)}, f32[2,2,1]{1,2,0:T(1,128)}, u32[]{:S(2)}) copy-start(f32[2,2,1]{1,2,0:T(1,128)} %param.19) | copy-start | bytes 52
  27.8 46.8 %copy-start.10 = (f32[2,8,1]{1,2,0:T(1,128)S(1)}, f32[2,8,1]{1,2,0:T(1,128)}, u32[]{:S(2)}) copy-start(f32[2,8,1]{1,2,0:T(1,128)} %param.23) | copy-start | bytes 196
  27.9 48.2 %copy-start.8 = (f32[2,8,1,128]{3,2,1,0:T(1,128)S(1)}, f32[2,8,1,128]{3,2,1,0:T(1,128)}, u32[]{:S(2)}) copy-start(f32[2,8,1,128]{3,2,1,0:T(1,128)} %param.22) | copy-start | bytes 24580
  29.6 58.1 %copy-start.5 = (bf16[2,128,1024]{2,1,0:T(8,128)(2,1)S(1)}, bf16[2,128,1024]{2,1,0:T(8,128)(2,1)}, u32[]{:S(2)}) copy-start(bf16[2,128,1024]{2,1,0:T(8,128)(2,1)} %param.20) | copy-start | bytes 1572868
  30.4 81.0 %all-gather.4.cloned.1.call-start = ((), (), s32[]{:S(2)}) async-start(), calls=%async_computation | async-start | bytes 1179648 | tf_op jit(solution)/shard_map/all_gather | solution.py:124
  88.6 70.3 %all-reduce.19.cloned.1.call-start = ((), (), s32[]{:S(2)}) async-start(), calls=%async_computation.2 | async-start | bytes 134144
  112.7 1.0 copy-start.1
  113.7 2.3 copy-start.4
  117.6 112.6 %all-reduce.17.cloned.1.call-start = ((), (), s32[]{:S(2)}) async-start(), calls=%async_computation.1 | async-start | bytes 262144
  117.6 0.7 copy-start.13
  159.0 0.7 copy-start.12
  159.7 0.6 copy-start.11
  163.8 10.1 %copy-start.6 = (bf16[2,128,1024]{2,1,0:T(8,128)(2,1)S(1)}, bf16[2,128,1024]{2,1,0:T(8,128)(2,1)}, u32[]{:S(2)}) copy-start(bf16[2,128,1024]{2,1,0:T(8,128)(2,1)} %param.20) | copy-start | bytes 1572868
Sparse Core Ops, SparseCore 0:
  30.5 42.6 all-reduce.20
  88.8 22.6 all-gather.3
  117.7 41.2 all-reduce.18
  174.8 55.3 all-reduce.16
